TPU v7x, 128 devices: a whole 4x4x4 slice. The times are simulated.
128 devices in a mesh: sp: 16 (over z, x), dp: 8 (over y, core).
Axes of the slice: x: 4, y: 4, z: 4, core: 2. Of those that a mesh axis runs over, the one named last changes fastest.
Arguments:
- hidden_in: bfloat16 [8, 2048, 2048], P('dp', 'sp'), may hold values from -6 to 6
- in_weight: bfloat16 [2048, 512], P(('sp', 'dp')), may hold values from -0.125 to 0.125
- lam_real: float32 [32, 64], replicated, may hold values from -4 to 0, as said below
- lam_imag: float32 [32, 64], replicated, may hold values from 1 to 200
- log_step: float32 [32], replicated, may hold values from -4.61 to -2.3
- b_real: float32 [32, 64, 16], replicated, may hold values from -1 to 1
- b_imag: float32 [32, 64, 16], replicated, may hold values from -1 to 1
- c_real: float32 [32, 16, 64], replicated, may hold values from -0.3 to 0.3
- c_imag: float32 [32, 16, 64], replicated, may hold values from -0.3 to 0.3
- skip_weight: float32 [512], replicated, may hold values from -4 to 4
- lin_weight: bfloat16 [512, 2048], P(None, ('sp', 'dp')), may hold values from -0.25 to 0.25
- gate_weight: bfloat16 [512, 2048], P(None, ('sp', 'dp')), may hold values from -0.25 to 0.25
Outputs:
- mixed: bfloat16 [8, 2048, 2048], P('dp', 'sp')
Inputs may be any that keep to these rules, and one draw needn't show every extreme that they name: `lam_real`: negative in every entry.
All inputs are finite; a program needn't handle non-finite values.
Results may differ from a plain program's by a relative error of at most 0.0047.
The roundings to bfloat16 on the way count: a program that leaves them out, or rounds other values in their place, can miss the bound.
Values may be sent and summed in bfloat16 or wider, within the bound.
A program may use at most 64 MiB of HBM per device.

v0:
```python
import math

import jax
import jax.numpy as jnp
from jax import lax
from jax.sharding import PartitionSpec as P


def rows_first(arrays, axis, dims):
    turned = [jnp.moveaxis(a, dim, 0) for a, dim in zip(arrays, dims)]
    widths = [t[0].size for t in turned]
    both = jnp.concatenate([t.reshape(-1, w) for t, w in zip(turned, widths)], axis=1)
    out = lax.all_gather(both, axis, axis=0, tiled=True)
    tiles = jnp.split(out, [sum(widths[:k]) for k in range(1, len(widths))], axis=1)
    return tuple(
        (
            jnp.moveaxis(b.reshape(-1, *t.shape[1:]), 0, dim)
            for b, t, dim in zip(tiles, turned, dims)
        )
    )


def step_factors(lam_real, lam_imag, log_step, b_real, b_imag):
    step = jnp.exp(log_step)[:, None]
    xpart = lam_real * step
    wpart = lam_imag * step
    decay_re = jnp.exp(xpart) * jnp.cos(wpart)
    decay_im = jnp.exp(xpart) * jnp.sin(wpart)
    numer_re = jnp.expm1(xpart) * jnp.cos(wpart) - 2.0 * jnp.sin(0.5 * wpart) ** 2
    magnitude = lam_real * lam_real + lam_imag * lam_imag
    ratio_re = (numer_re * lam_real + decay_im * lam_imag) / magnitude
    ratio_im = (decay_im * lam_real - numer_re * lam_imag) / magnitude
    bbar_re = ratio_re[..., None] * b_real - ratio_im[..., None] * b_imag
    bbar_im = ratio_re[..., None] * b_imag + ratio_im[..., None] * b_real
    return (decay_re, decay_im, bbar_re, bbar_im)


def combine(left, right):
    lre, lim, lbre, lbim = left
    rre, rim, rbre, rbim = right
    return (
        rre * lre - rim * lim,
        rre * lim + rim * lre,
        rre * lbre - rim * lbim + rbre,
        rre * lbim + rim * lbre + rbim,
    )


def block_scan(piece, factors):
    decay_re, decay_im, bbar_re, bbar_im = factors
    highest = lax.Precision.HIGHEST
    block = piece.shape[0]
    groups_here, states = decay_re.shape
    lanes = groups_here * states
    source = piece.astype(jnp.float32)
    shaped = source.reshape(block, groups_here, source.shape[1] // groups_here)
    drive_re = jnp.einsum("tgh,gph->tgp", shaped, bbar_re, precision=highest).reshape(block, lanes)
    drive_im = jnp.einsum("tgh,gph->tgp", shaped, bbar_im, precision=highest).reshape(block, lanes)
    are = jnp.broadcast_to(decay_re.reshape(lanes), drive_re.shape)
    aim = jnp.broadcast_to(decay_im.reshape(lanes), drive_re.shape)
    return (source, lax.associative_scan(combine, (are, aim, drive_re, drive_im), axis=0))


def run_blocks(sequence, factors, out_re, out_im, direct, start):
    highest = lax.Precision.HIGHEST
    length, width = sequence.shape
    block = math.gcd(length, 512)
    blocks = sequence.reshape(length // block, block, width)
    groups_here, states = factors[0].shape

    def block_step(carry, piece):
        carry_re, carry_im = carry
        source, scanned = block_scan(piece, factors)
        cum_re, cum_im, local_re, local_im = scanned
        state_re = local_re + cum_re * carry_re - cum_im * carry_im
        state_im = local_im + cum_re * carry_im + cum_im * carry_re
        summed = jnp.einsum(
            "tgp,ghp->tgh", state_re.reshape(block, groups_here, states), out_re, precision=highest
        ) - jnp.einsum(
            "tgp,ghp->tgh", state_im.reshape(block, groups_here, states), out_im, precision=highest
        )
        result = jax.nn.gelu(summed.reshape(block, width) + direct * source)
        return ((state_re[-1], state_im[-1]), result.astype(jnp.bfloat16))

    _, results = lax.scan(block_step, start, blocks)
    return results.reshape(length, width)


def by_groups(sequence, lam_real, lam_imag, log_step, b_real, b_imag, c_real, c_imag, skip_weight):
    per_group = b_real.shape[2]
    groups_here = sequence.shape[1] // per_group
    first = lax.axis_index("sp") * groups_here
    pick = lambda table: lax.dynamic_slice_in_dim(table, first, groups_here, 0)
    factors = step_factors(
        pick(lam_real), pick(lam_imag), pick(log_step), pick(b_real), pick(b_imag)
    )
    direct = lax.dynamic_slice_in_dim(skip_weight, first * per_group, groups_here * per_group, 0)
    zeros = jnp.zeros((factors[0].size,), jnp.float32)
    return run_blocks(sequence, factors, pick(c_real), pick(c_imag), direct, (zeros, zeros))


def shards(
    hidden_in,
    in_weight,
    lam_real,
    lam_imag,
    log_step,
    b_real,
    b_imag,
    c_real,
    c_imag,
    skip_weight,
    lin_weight,
    gate_weight,
):
    tok_rows = hidden_in[0]
    whole_in, whole_lin, whole_gate = rows_first(
        (in_weight, lin_weight, gate_weight), ("sp", "dp"), (0, 1, 1)
    )
    inputs = jnp.dot(tok_rows, whole_in, preferred_element_type=jnp.float32).astype(jnp.bfloat16)
    sequence = lax.all_to_all(inputs, "sp", split_axis=1, concat_axis=0, tiled=True)
    mixer_local = by_groups(
        sequence, lam_real, lam_imag, log_step, b_real, b_imag, c_real, c_imag, skip_weight
    )
    mixer_out = lax.all_to_all(mixer_local, "sp", split_axis=0, concat_axis=1, tiled=True)
    linear = jnp.dot(mixer_out, whole_lin, preferred_element_type=jnp.float32)
    gate = jnp.dot(mixer_out, whole_gate, preferred_element_type=jnp.float32)
    mixed = (linear * jax.nn.sigmoid(gate)).astype(jnp.bfloat16)
    return mixed[None]


def solution(mesh):
    placed = (
        P("dp", "sp", None),
        P(("sp", "dp"), None),
        P(),
        P(),
        P(),
        P(),
        P(),
        P(),
        P(),
        P(),
        P(None, ("sp", "dp")),
        P(None, ("sp", "dp")),
    )
    return jax.shard_map(
        shards, mesh=mesh, in_specs=placed, out_specs=P("dp", "sp", None), check_vma=False
    )
```

profile of v0, /device:TPU:1, one launch (start us, length us, event | category | flops | bytes accessed | tf_op | source)
XLA Modules:
  0.0 266.9 jit_solution(9730837093817101557)
XLA Ops:
  6.5 1.4 pad_maximum_fusion.32
  8.0 0.7 dynamic-slice_exponential_fusion
  8.7 0.8 multiply_subtract_fusion.10
  9.8 0.8 add_divide_fusion
  10.8 0.5 multiply_subtract_fusion.17
  11.3 0.7 multiply_add_fusion.9
  12.0 70.3 %all-gather.2.cloned.1.call-done = bf16[2048,1536]{1,0:T(8,128)(2,1)} async-done(((bf16[16,1536]{1,0:T(8,128)(2,1)}), bf16[2048,1536]{1,0:T(8,128)(2,1)}) %all-gather.2.cloned.1.call-update) | async-done | bytes 6291472 | tf_op jit(solution)/shard_map/all_gather | solution.py:13
  82.3 3.0 %fusion.18 = bf16[512,128]{1,0:T(8,128)(2,1)} fusion(bf16[2048,1536]{1,0:T(8,128)(2,1)} %all-gather.2.cloned.1.call-done, bf16[1,128,2048]{2,1,0:T(8,128)(2,1)S(1)} %copy-done), kind=kOutput, calls=%fused_computation.136 | convolution fusion | flops 268500992 | bytes 2752512 | tf_op jit(solution)/shard_map/dot_general | solution.py:120
  85.3 4.1 %all-to-all-start = ((bf16[128,16,32]{0,2,1:T(8,128)(2,1)}), bf16[128,16,32]{0,2,1:T(8,128)(2,1)S(1)}, u32[]{:S(2)}, u32[]{:S(2)}) async-start(bf16[128,16,32]{0,2,1:T(8,128)(2,1)} %bitcast.33), calls=%async_computation | async-start | bytes 262144 | tf_op jit(solution)/shard_map/all_to_all | solution.py:121
  89.6 0.6 slice.1182
  90.3 1.3 dynamic_slice.38
  91.6 0.7 constant_dynamic-slice_fusion.1
  92.3 3.9 %all-to-all-done = bf16[128,16,32]{0,2,1:T(8,128)(2,1)S(1)} async-done(((bf16[128,16,32]{0,2,1:T(8,128)(2,1)}), bf16[128,16,32]{0,2,1:T(8,128)(2,1)S(1)}, u32[]{:S(2)}, u32[]{:S(2)}) %all-to-all-start) | async-done | bytes 131104 | tf_op jit(solution)/shard_map/all_to_all | solution.py:121
  96.4 0.5 broadcast_in_dim.7.clone
  97.4 146.8 %while.18 = (s32[]{:T(128)}, f32[128]{0:T(128)}, f32[128]{0:T(128)}, bf16[4,512,32]{1,2,0:T(8,128)(2,1)S(1)}, bf16[4,512,32]{1,2,0:T(8,128)(2,1)S(1)}, /*index=5...) while((s32[]{:T(128)}, f32[128]{0:T(128)}, ...), condition=%wide.wide.region_1.2_spmd, body=%wide.wide.region_0.1_spmd.sunk | while | flops 53527552 | bytes 26572484 | solution.py:85
  97.4 0.6 pad_add_fusion.9
  98.6 4.5 %slice.1651 = f32[255,128]{0,1:T(8,128)S(1)} slice(f32[512,128]{0,1:T(8,128)S(1)} %bitcast.197), slice={[2:512:2], [0:128:1]} | slice | bytes 261120 | tf_op jit(solution)/shard_map/while/body/eval_jaxpr/slice | solution.py:61
  103.2 4.5 %slice.1598 = f32[256,128]{0,1:T(8,128)S(1)} slice(f32[512,128]{0,1:T(8,128)S(1)} %bitcast.198), slice={[1:512:2], [0:128:1]} | slice | bytes 262144 | tf_op jit(solution)/shard_map/while/body/eval_jaxpr/slice | solution.py:61
  107.7 4.5 %slice.1596 = f32[256,128]{0,1:T(8,128)S(1)} slice(f32[512,128]{0,1:T(8,128)S(1)} %bitcast.199), slice={[0:511:2], [0:128:1]} | slice | bytes 262144 | tf_op jit(solution)/shard_map/while/body/eval_jaxpr/slice | solution.py:61
  112.9 4.5 %slice.1597 = f32[256,128]{0,1:T(8,128)S(1)} slice(f32[512,128]{0,1:T(8,128)S(1)} %bitcast.193), slice={[0:511:2], [0:128:1]} | slice | bytes 262144 | tf_op jit(solution)/shard_map/while/body/eval_jaxpr/slice | solution.py:61
  117.4 4.5 %slice.1595 = f32[256,128]{0,1:T(8,128)S(1)} slice(f32[512,128]{0,1:T(8,128)S(1)} %bitcast.194), slice={[1:512:2], [0:128:1]} | slice | bytes 262144 | tf_op jit(solution)/shard_map/while/body/eval_jaxpr/slice | solution.py:61
  121.9 4.5 %slice.1594 = f32[255,128]{0,1:T(8,128)S(1)} slice(f32[512,128]{0,1:T(8,128)S(1)} %bitcast.195), slice={[2:512:2], [0:128:1]} | slice | bytes 261120 | tf_op jit(solution)/shard_map/while/body/eval_jaxpr/slice | solution.py:61
  129.8 0.6 pad_maximum_fusion.126
  130.7 0.8 multiply_add_fusion.31
  131.5 0.5 slice_bitcast_fusion.6
  132.4 0.5 slice_bitcast_fusion.7
  133.3 0.8 fusion.70
  134.1 0.6 pad_add_fusion.9
  135.3 4.5 %slice.1651 = f32[255,128]{0,1:T(8,128)S(1)} slice(f32[512,128]{0,1:T(8,128)S(1)} %bitcast.197), slice={[2:512:2], [0:128:1]} | slice | bytes 261120 | tf_op jit(solution)/shard_map/while/body/eval_jaxpr/slice | solution.py:61
  139.8 4.5 %slice.1598 = f32[256,128]{0,1:T(8,128)S(1)} slice(f32[512,128]{0,1:T(8,128)S(1)} %bitcast.198), slice={[1:512:2], [0:128:1]} | slice | bytes 262144 | tf_op jit(solution)/shard_map/while/body/eval_jaxpr/slice | solution.py:61
  144.3 4.5 %slice.1596 = f32[256,128]{0,1:T(8,128)S(1)} slice(f32[512,128]{0,1:T(8,128)S(1)} %bitcast.199), slice={[0:511:2], [0:128:1]} | slice | bytes 262144 | tf_op jit(solution)/shard_map/while/body/eval_jaxpr/slice | solution.py:61
  149.5 4.5 %slice.1597 = f32[256,128]{0,1:T(8,128)S(1)} slice(f32[512,128]{0,1:T(8,128)S(1)} %bitcast.193), slice={[0:511:2], [0:128:1]} | slice | bytes 262144 | tf_op jit(solution)/shard_map/while/body/eval_jaxpr/slice | solution.py:61
  154.1 4.5 %slice.1595 = f32[256,128]{0,1:T(8,128)S(1)} slice(f32[512,128]{0,1:T(8,128)S(1)} %bitcast.194), slice={[1:512:2], [0:128:1]} | slice | bytes 262144 | tf_op jit(solution)/shard_map/while/body/eval_jaxpr/slice | solution.py:61
  158.6 4.5 %slice.1594 = f32[255,128]{0,1:T(8,128)S(1)} slice(f32[512,128]{0,1:T(8,128)S(1)} %bitcast.195), slice={[2:512:2], [0:128:1]} | slice | bytes 261120 | tf_op jit(solution)/shard_map/while/body/eval_jaxpr/slice | solution.py:61
  166.5 0.6 pad_maximum_fusion.126
  167.4 0.8 multiply_add_fusion.31
  168.2 0.5 slice_bitcast_fusion.6
  169.1 0.5 slice_bitcast_fusion.7
  170.0 0.8 fusion.70
  170.8 0.6 pad_add_fusion.9
  172.0 4.5 %slice.1651 = f32[255,128]{0,1:T(8,128)S(1)} slice(f32[512,128]{0,1:T(8,128)S(1)} %bitcast.197), slice={[2:512:2], [0:128:1]} | slice | bytes 261120 | tf_op jit(solution)/shard_map/while/body/eval_jaxpr/slice | solution.py:61
  176.5 4.5 %slice.1598 = f32[256,128]{0,1:T(8,128)S(1)} slice(f32[512,128]{0,1:T(8,128)S(1)} %bitcast.198), slice={[1:512:2], [0:128:1]} | slice | bytes 262144 | tf_op jit(solution)/shard_map/while/body/eval_jaxpr/slice | solution.py:61
  181.0 4.5 %slice.1596 = f32[256,128]{0,1:T(8,128)S(1)} slice(f32[512,128]{0,1:T(8,128)S(1)} %bitcast.199), slice={[0:511:2], [0:128:1]} | slice | bytes 262144 | tf_op jit(solution)/shard_map/while/body/eval_jaxpr/slice | solution.py:61
  186.2 4.5 %slice.1597 = f32[256,128]{0,1:T(8,128)S(1)} slice(f32[512,128]{0,1:T(8,128)S(1)} %bitcast.193), slice={[0:511:2], [0:128:1]} | slice | bytes 262144 | tf_op jit(solution)/shard_map/while/body/eval_jaxpr/slice | solution.py:61
  190.8 4.5 %slice.1595 = f32[256,128]{0,1:T(8,128)S(1)} slice(f32[512,128]{0,1:T(8,128)S(1)} %bitcast.194), slice={[1:512:2], [0:128:1]} | slice | bytes 262144 | tf_op jit(solution)/shard_map/while/body/eval_jaxpr/slice | solution.py:61
  195.3 4.5 %slice.1594 = f32[255,128]{0,1:T(8,128)S(1)} slice(f32[512,128]{0,1:T(8,128)S(1)} %bitcast.195), slice={[2:512:2], [0:128:1]} | slice | bytes 261120 | tf_op jit(solution)/shard_map/while/body/eval_jaxpr/slice | solution.py:61
  203.2 0.6 pad_maximum_fusion.126
  204.1 0.8 multiply_add_fusion.31
  205.8 0.5 slice_bitcast_fusion.7
  206.7 0.8 fusion.70
  207.5 0.6 pad_add_fusion.9
  208.7 4.5 %slice.1651 = f32[255,128]{0,1:T(8,128)S(1)} slice(f32[512,128]{0,1:T(8,128)S(1)} %bitcast.197), slice={[2:512:2], [0:128:1]} | slice | bytes 261120 | tf_op jit(solution)/shard_map/while/body/eval_jaxpr/slice | solution.py:61
  213.2 4.5 %slice.1598 = f32[256,128]{0,1:T(8,128)S(1)} slice(f32[512,128]{0,1:T(8,128)S(1)} %bitcast.198), slice={[1:512:2], [0:128:1]} | slice | bytes 262144 | tf_op jit(solution)/shard_map/while/body/eval_jaxpr/slice | solution.py:61
  217.7 4.5 %slice.1596 = f32[256,128]{0,1:T(8,128)S(1)} slice(f32[512,128]{0,1:T(8,128)S(1)} %bitcast.199), slice={[0:511:2], [0:128:1]} | slice | bytes 262144 | tf_op jit(solution)/shard_map/while/body/eval_jaxpr/slice | solution.py:61
  222.9 4.5 %slice.1597 = f32[256,128]{0,1:T(8,128)S(1)} slice(f32[512,128]{0,1:T(8,128)S(1)} %bitcast.193), slice={[0:511:2], [0:128:1]} | slice | bytes 262144 | tf_op jit(solution)/shard_map/while/body/eval_jaxpr/slice | solution.py:61
  227.5 4.5 %slice.1595 = f32[256,128]{0,1:T(8,128)S(1)} slice(f32[512,128]{0,1:T(8,128)S(1)} %bitcast.194), slice={[1:512:2], [0:128:1]} | slice | bytes 262144 | tf_op jit(solution)/shard_map/while/body/eval_jaxpr/slice | solution.py:61
  232.0 4.5 %slice.1594 = f32[255,128]{0,1:T(8,128)S(1)} slice(f32[512,128]{0,1:T(8,128)S(1)} %bitcast.195), slice={[2:512:2], [0:128:1]} | slice | bytes 261120 | tf_op jit(solution)/shard_map/while/body/eval_jaxpr/slice | solution.py:61
  239.9 0.6 pad_maximum_fusion.126
  240.8 0.8 multiply_add_fusion.31
  242.5 0.5 slice_bitcast_fusion.7
  243.4 0.8 fusion.70
  244.4 9.9 %all_to_all.35 = bf16[16,128,32]{1,2,0:T(8,128)(2,1)S(1)} all-to-all(bf16[16,128,32]{1,2,0:T(8,128)(2,1)S(1)} %copy.44), channel_id=1, replica_groups=mesh['sp'=16,'dp'=8] {'sp'}, dimensions={0} | all-to-all | bytes 262144 | tf_op jit(solution)/shard_map/all_to_all | solution.py:125
  254.3 2.5 fusion.11
  256.8 3.2 %fusion.13 = bf16[1,128,2048]{2,1,0:T(8,128)(2,1)} fusion(f32[128,2048]{1,0:T(8,128)S(1)} %fusion.11, bf16[128,512]{0,1:T(8,128)(2,1)S(1)} %bitcast.207, bf16[2048,1536]{1,0:T(8,128)(2,1)} %all-gather.2.cloned.1.call-done), kind=kOutput, calls=%fused_computation.131 | convolution fusion | flops 268959744 | bytes 3801088 | tf_op jit(solution)/shard_map/dot_general | solution.py:126
  (888 shorter events, 20.9 us)
Async XLA Ops:
  6.5 75.8 %copy-start = (bf16[1,128,2048]{2,1,0:T(8,128)(2,1)S(1)}, bf16[1,128,2048]{2,1,0:T(8,128)(2,1)}, u32[]{:S(2)}) copy-start(bf16[1,128,2048]{2,1,0:T(8,128)(2,1)} %param.14) | copy-start | bytes 1572868
  6.5 75.8 %all-gather.2.cloned.1.call-start = ((), (), s32[]{:S(2)}) async-start(), calls=%async_computation.2 | async-start | bytes 6340608 | tf_op jit(solution)/shard_map/all_gather | solution.py:13
  9.6 80.7 %copy-start.1 = (f32[2,64]{1,0:T(2,128)}, f32[2,64]{1,0:T(2,128)S(1)}, u32[]{:S(2)}) copy-start(f32[2,64]{1,0:T(2,128)S(1)} %get-tuple-element.1126) | copy-start | bytes 1540
  9.6 80.7 %copy-start.2 = (f32[2,64]{1,0:T(2,128)}, f32[2,64]{1,0:T(2,128)S(1)}, u32[]{:S(2)}) copy-start(f32[2,64]{1,0:T(2,128)S(1)} %get-tuple-element.1125) | copy-start | bytes 1540
  85.3 10.9 %all-to-all-start = ((bf16[128,16,32]{0,2,1:T(8,128)(2,1)}), bf16[128,16,32]{0,2,1:T(8,128)(2,1)S(1)}, u32[]{:S(2)}, u32[]{:S(2)}) async-start(bf16[128,16,32]{0,2,1:T(8,128)(2,1)} %bitcast.33), calls=%async_computation | async-start | bytes 262144 | tf_op jit(solution)/shard_map/all_to_all | solution.py:121
Sparse Core Ops, SparseCore 0:
  10.4 71.8 all-gather.1
where the time goes:
time: 269 us; the launch traced here: 267 us
  local copies, waits for them, and re-layouts  127 us (47%)
  waiting for transfers between devices  74.2 us (28%)
  other arithmetic  19.4 us (7%)
  between operations  13.5 us (5%)
  matrix products  13.3 us (5%)
  blocking collectives  9.92 us (4%)
  loops' own time  5.28 us (2%)
  starting transfers between devices  4.08 us (2%)
    slice x250, local copies, waits for them, and re-layouts, block_scan(): lax.associative_scan(combine, (are, aim, drive_re, drive_im), axis=0)  112 us
    all_gather x1, waiting for transfers between devices, rows_first(): out = lax.all_gather(both, axis, axis=0, tiled=True)  70.3 us
    all_to_all x1, blocking collectives, shards(): lax.all_to_all(mixer_local, 'sp', split_axis=0, concat_axis=1, tiled=True)  9.92 us
  transfers between devices with their start and end apart: 2, of which 2 were waited for; matrix products, arithmetic and copies ran while one was open for 3% of the time, Pallas kernels for 0%

commit v1 on v0

v1 whole, which is shorter than its diff:
```python
import functools

import jax
import jax.numpy as jnp
from jax import lax
from jax.experimental import pallas as pl
from jax.experimental.pallas import tpu as pltpu
from jax.sharding import PartitionSpec as P

MESH = pl.DeviceIdType.MESH
ANY = pl.ANY
HIGH = lax.Precision.HIGHEST
NT = (((1,), (1,)), ((), ()))
F32, BF16 = jnp.float32, jnp.bfloat16

TOK = 128
GRP = 16
TILES = 8
STR = 136
SEQ = 2 * TILES * STR

ITEMS = (
    ("w", 0, 0, (2, 1, 0)),
    ("w", 1, 0, (2, 0, 1)),
    ("l", None, 0, (1, 0, 2)),
    ("l", None, 256, (0, 1, 2)),
    ("g", None, 0, (1, 2, 0)),
    ("g", None, 256, (0, 2, 1)),
)
PER_ITEM = 12


def split(a):
    high = a.astype(BF16)
    return high, (a - high.astype(F32)).astype(BF16)


def kernel(
    hid, win, lamr, lami, lst, br, bi, cr, ci, skip, lin, gate, out,
    hbuf, wbuf, lbuf, gbuf, drive, bh, bl, ch, cl, ubuf,
    lamv, lstv, bv, cv, skv, linv, gatev, fbuf, fsend, msend, mbuf, obuf,
    loc, rs, rr, hs, hr, ws, wr, fs, fr, ms, mr, ds_, dr_, os_,
):
    sp, dp = lax.axis_index("sp"), lax.axis_index("dp")
    z, x, y, h = lax.div(sp, 4), lax.rem(sp, 4), lax.div(dp, 2), lax.rem(dp, 2)
    at = (z, x, y)
    other = 1 - h
    peer = (sp, y * 2 + other)

    def device(pos):
        return (pos[0] * 4 + pos[1], pos[2] * 2 + h)

    def moved(axis, by):
        pos = list(at)
        pos[axis] = lax.rem(at[axis] + by + 4, 4)
        return device(pos)

    def remote(src, dst, send, recv, to):
        return pltpu.make_async_remote_copy(
            src_ref=src, dst_ref=dst, send_sem=send, recv_sem=recv, device_id=to, device_id_type=MESH
        )

    half_rows = pl.ds(h * GRP, GRP)
    half_cols = pl.ds(pl.multiple_of(h * 256, 256), 256)
    other_cols = pl.ds(pl.multiple_of(other * 256, 256), 256)
    loads = [
        (win.at[:, half_cols], wbuf.at[z, x, y, h]),
        (lin, linv),
        (gate, gatev),
        (hid.at[0], hbuf.at[h]),
        (lamr.at[half_rows], lamv.at[0]),
        (lami.at[half_rows], lamv.at[1]),
        (br.at[half_rows], bv.at[0]),
        (bi.at[half_rows], bv.at[1]),
        (cr.at[half_rows], cv.at[0]),
        (ci.at[half_rows], cv.at[1]),
        (skip.at[:, half_cols], skv),
        (lst, lstv),
    ]
    loads = [pltpu.make_async_copy(s, d, loc.at[k]) for k, (s, d) in enumerate(loads)]
    for c in loads:
        c.start()

    barrier = pltpu.get_barrier_semaphore()
    pl.semaphore_signal(barrier, inc=1, device_id=peer, device_id_type=MESH)
    for k in range(1, 4):
        pl.semaphore_signal(barrier, inc=1, device_id=moved(2, k), device_id_type=MESH)
    for k in range(1, 16):
        pl.semaphore_signal(barrier, inc=1, device_id=(lax.rem(sp + k, 16), dp), device_id_type=MESH)
    pl.semaphore_wait(barrier, 19)

    w_pair = remote(win.at[:, other_cols], wbuf.at[z, x, y, h], ws, wr, peer)
    w_pair.start()
    h_pair = remote(hid.at[0], hbuf.at[h], hs, hr, peer)
    h_pair.start()

    bufs = {"w": wbuf, "l": lbuf, "g": gbuf}

    def slab(item, phase, i, cols=None):
        name, core, first, order = ITEMS[item]
        idx = [at[a] for a in range(3)]
        for a in order[: phase - 1]:
            idx[a] = slice(None)
        idx[order[phase - 1]] = i
        start, width = cols if cols is not None else (0, 256)
        return bufs[name].at[
            idx[0], idx[1], idx[2], h if core is None else core, :, pl.ds(first + start, width)
        ]

    def turn(axis, by):
        return lax.rem(at[axis] + by + 4, 4)

    def direct(item, phase):
        axis = ITEMS[item][3][phase - 1]
        copies = []
        for k in range(1, 4):
            sem = item * PER_ITEM + (phase - 1) * 3 + k - 1
            own = slab(item, phase, at[axis])
            copies.append(remote(own, own, rs.at[sem], rr.at[sem], moved(axis, k)))
        return copies

    H0, H1 = (0, 128), (128, 128)

    def last(item):
        axis = ITEMS[item][3][2]
        sem = item * PER_ITEM + 6
        plan = (
            (0, H0, 1), (0, H1, -1), (0, H1, 1), (0, H0, -1), (-1, H0, 1), (1, H1, -1),
        )
        copies = []
        for k, (which, cols, by) in enumerate(plan):
            piece = slab(item, 3, turn(axis, which), cols)
            copies.append(remote(piece, piece, rs.at[sem + k], rr.at[sem + k], moved(axis, by)))
        return copies

    first, second, third = {}, {}, {}
    for i in range(6):
        first[i], second[i], third[i] = direct(i, 1), direct(i, 2), last(i)

    passed = {}

    def pass_on(item, which):
        axis = ITEMS[item][3][2]
        piece = slab(item, 3, turn(axis, which))
        sem = (item - 2) * 4 + which + 1
        passed[sem] = remote(piece, piece, ds_.at[sem], dr_.at[sem], peer)
        passed[sem].start()

    def start(copies):
        for c in copies:
            c.start()

    def arrived(copies):
        for c in copies:
            c.wait_recv()

    loads[0].wait()
    w_pair.wait_recv()
    start(first[0])
    start(first[1])

    eye = (
        lax.broadcasted_iota(jnp.int32, (16, 16), 0) == lax.broadcasted_iota(jnp.int32, (16, 16), 1)
    ).astype(F32)
    for k, (stage, buf) in enumerate(((linv, lbuf), (gatev, gbuf))):
        loads[1 + k].wait()
        turned = lax.dot_general(eye.astype(BF16), stage[...], NT, preferred_element_type=F32)
        buf[z, x, y, h] = turned.astype(BF16)
    for i in range(2, 6):
        start(first[i])

    for c in loads[4:]:
        c.wait()
    row8 = lax.broadcasted_iota(jnp.int32, (8, 128), 0)
    lane8 = lax.broadcasted_iota(jnp.int32, (8, 128), 1)
    log_step = jnp.zeros((8, 128), F32)
    for g in range(GRP):
        here = (row8 == g // 2) & ((lane8 >= 64) == (g % 2 == 1))
        log_step = jnp.where(here, lstv[h * GRP + g], log_step)

    def pairs(k):
        both = [lamv[k, pl.ds(q, 8, stride=2), :] for q in range(2)]
        return jnp.concatenate(both, axis=1)

    lam_re, lam_im = pairs(0), pairs(1)
    step = jnp.exp(log_step)
    xpart = lam_re * step
    wpart = lam_im * step
    ex = jnp.exp(xpart)
    cosw, sinw, sinh_ = jnp.cos(wpart), jnp.sin(wpart), jnp.sin(0.5 * wpart)
    a_re, a_im = ex * cosw, ex * sinw
    plain = ex == 1.0
    em1 = jnp.where(plain, xpart, (ex - 1.0) * xpart / jnp.log(jnp.where(plain, 2.0, ex)))
    num_re = em1 * cosw - 2.0 * sinh_ * sinh_
    size = lam_re * lam_re + lam_im * lam_im
    ratio_re = (num_re * lam_re + a_im * lam_im) / size
    ratio_im = (a_im * lam_re - num_re * lam_im) / size
    p_re, p_im = a_re, a_im
    for _ in range(7):
        p_re, p_im = p_re * p_re - p_im * p_im, 2.0 * p_re * p_im

    for i in (0, 1):
        arrived(first[i])
        start(second[i])

    turned = [
        lax.dot_general(eye, bv[k].reshape(GRP * 64, 16), NT, precision=HIGH, preferred_element_type=F32)
        for k in range(2)
    ]
    low = lax.broadcasted_iota(jnp.int32, (16, 128), 1) < 64
    bh[...] = jnp.zeros_like(bh)
    bl[...] = jnp.zeros_like(bl)
    for j in range(TILES):
        b_re, b_im = (t[:, 128 * j : 128 * j + 128] for t in turned)
        r_re, r_im = ratio_re[j : j + 1], ratio_im[j : j + 1]
        for k, part in enumerate((r_re * b_re - r_im * b_im, r_re * b_im + r_im * b_re)):
            block = jnp.concatenate([jnp.where(low, part, 0.0), jnp.where(low, 0.0, part)], axis=0)
            rows = slice(32 * (j % 4), 32 * (j % 4) + 32)
            bh[j, rows, 128 * k : 128 * k + 128], bl[j, rows, 128 * k : 128 * k + 128] = split(block)

    for i in (0, 1):
        arrived(second[i])
        start(third[i][:4])
    for i in (4, 5, 2, 3):
        arrived(first[i])
        start(second[i])

    rows_c = lax.broadcasted_iota(jnp.int32, (128, 128), 0)
    lanes_c = lax.broadcasted_iota(jnp.int32, (128, 128), 1)
    same = lax.rem(lax.div(rows_c, 16), 2) == lax.div(lanes_c, 64)
    pair_of = lax.div(rows_c, 32)
    for a in range(2):
        for k, sign in ((0, 1.0), (1, -1.0)):
            c = cv[k, 8 * a : 8 * a + 8].reshape(128, 64) * sign
            c = jnp.where(same, jnp.concatenate([c, c], axis=1), 0.0)
            for j in range(4):
                cols = slice(256 * j + 128 * k, 256 * j + 128 * k + 128)
                ch[a, :, cols], cl[a, :, cols] = split(jnp.where(pair_of == j, c, 0.0))

    for k in (0, 1):
        for i in (0, 1):
            third[i][k].wait_recv()
            third[i][4 + k].start()
    for i in (4, 5):
        arrived(second[i])
        start(third[i][:4])
        pass_on(i, 0)
    for i in (0, 1):
        arrived(third[i][2:])
    for i in (2, 3):
        arrived(second[i])
        start(third[i][:4])
        pass_on(i, 0)

    loads[3].wait()
    h_pair.wait_recv()
    u = jnp.dot(
        hbuf[...].reshape(2 * TOK, 2048), wbuf[...].reshape(2048, 256), preferred_element_type=F32
    ).astype(BF16)
    ubuf[...] = u
    for j in range(TILES):
        cols = u[:, 128 * (j // 4) : 128 * (j // 4) + 128]
        d = jnp.dot(cols, bh[j], preferred_element_type=F32)
        d += jnp.dot(cols, bl[j], preferred_element_type=F32)
        for s in range(2):
            for k in range(2):
                rows = pl.ds(s * SEQ + (k * TILES + j) * STR, TOK)
                drive[rows, :] = d[TOK * s : TOK * s + TOK, 128 * k : 128 * k + 128]

    def scan(init, keep):
        def body(i, carry):
            carry = list(carry)
            for n in range(8):
                t = i * 8 + n
                for s in range(2):
                    at_re = pl.ds(s * SEQ + t, TILES, stride=STR)
                    at_im = pl.ds(s * SEQ + TILES * STR + t, TILES, stride=STR)
                    re, im = carry[2 * s], carry[2 * s + 1]
                    carry[2 * s] = a_re * re - a_im * im + drive[at_re, :]
                    carry[2 * s + 1] = a_re * im + a_im * re + drive[at_im, :]
                    if keep:
                        drive[at_re, :] = carry[2 * s]
                        drive[at_im, :] = carry[2 * s + 1]
            return tuple(carry)

        return lax.fori_loop(0, TOK // 8, body, init)

    zero = jnp.zeros((8, 128), F32)
    ends = scan((zero,) * 4, False)
    for k in range(4):
        fsend[k] = ends[k]

    def to_later(k):
        return remote(fsend, fbuf.at[sp], fs.at[k], fr.at[sp], (lax.rem(sp + k, 16), dp))

    for k in range(1, 16):

        @pl.when(sp + k < 16)
        def _():
            to_later(k).start()

    for i in (4, 5, 2, 3):
        for k in (0, 1):
            third[i][k].wait_recv()
            third[i][4 + k].start()
    for i in (4, 5, 2, 3):
        arrived(third[i][2:4])
        pass_on(i, -1)
        pass_on(i, 1)

    def fold(j, carry):
        remote(fsend, fbuf.at[j], fs.at[0], fr.at[j], peer).wait_recv()
        new = []
        for s in range(2):
            re, im = carry[2 * s], carry[2 * s + 1]
            new.append(p_re * re - p_im * im + fbuf[j, 2 * s])
            new.append(p_re * im + p_im * re + fbuf[j, 2 * s + 1])
        return tuple(new)

    scan(lax.fori_loop(0, sp, fold, (zero,) * 4), True)

    for a in range(2):
        tiles = []
        for j in range(4):
            for k in range(2):
                rows = [pl.ds(s * SEQ + (k * TILES + 4 * a + j) * STR, TOK) for s in range(2)]
                tiles.append(jnp.concatenate([drive[r, :] for r in rows], axis=0))
        s_high, s_low = split(jnp.concatenate(tiles, axis=1))
        summed = lax.dot_general(s_high, ch[a], NT, preferred_element_type=F32)
        summed += lax.dot_general(s_low, ch[a], NT, preferred_element_type=F32)
        summed += lax.dot_general(s_high, cl[a], NT, preferred_element_type=F32)
        cols = slice(128 * a, 128 * a + 128)
        mixer = jax.nn.gelu(summed + skv[:, cols] * ubuf[:, cols].astype(F32)).astype(BF16)
        mine = jnp.where(h == 0, mixer[:TOK].astype(F32), mixer[TOK:].astype(F32)).astype(BF16)
        theirs = jnp.where(h == 0, mixer[TOK:].astype(F32), mixer[:TOK].astype(F32)).astype(BF16)
        mbuf[h, :, cols] = mine
        msend[:, cols] = theirs
    m_pair = remote(msend, mbuf.at[h], ms, mr, peer)
    m_pair.start()

    for i in (4, 5, 2, 3):
        arrived(third[i][4:])
        pass_on(i, 2)
    m_pair.wait_recv()
    for sem in sorted(passed):
        passed[sem].wait_recv()

    m = jnp.concatenate([mbuf[0], mbuf[1]], axis=1)
    puts = []
    for n in range(8):
        rows = (n // 2, slice(2 * (n % 2), 2 * (n % 2) + 2))
        linear = lax.dot_general(m, lbuf[rows].reshape(256, 512), NT, preferred_element_type=F32)
        gated = lax.dot_general(m, gbuf[rows].reshape(256, 512), NT, preferred_element_type=F32)
        cols = slice(256 * n, 256 * n + 256)
        obuf[:, cols] = (linear * jax.nn.sigmoid(gated)).astype(BF16)
        puts.append(
            pltpu.make_async_copy(obuf.at[:, pl.ds(256 * n, 256)], out.at[0, :, pl.ds(256 * n, 256)], os_.at[n])
        )
        puts[-1].start()

    for i in range(6):
        for c in first[i] + second[i] + third[i]:
            c.wait_send()
    for sem in sorted(passed):
        passed[sem].wait_send()
    for c in (w_pair, h_pair, m_pair):
        c.wait_send()
    for k in range(1, 16):

        @pl.when(sp + k < 16)
        def _():
            to_later(k).wait_send()

    for c in puts:
        c.wait()


def shards(hid, win, lamr, lami, lst, br, bi, cr, ci, skip, lin, gate):
    dma = pltpu.SemaphoreType.DMA
    vmem = pltpu.VMEM
    return pl.pallas_call(
        kernel,
        name="mixer",
        out_shape=jax.ShapeDtypeStruct((1, TOK, 2048), BF16),
        in_specs=[pl.BlockSpec(memory_space=ANY)] * 12,
        out_specs=pl.BlockSpec(memory_space=ANY),
        scratch_shapes=[
            vmem((2, TOK, 2048), BF16),
            vmem((4, 4, 4, 2, 16, 256), BF16),
            vmem((4, 4, 4, 2, 16, 512), BF16),
            vmem((4, 4, 4, 2, 16, 512), BF16),
            vmem((2 * SEQ, 128), F32),
            vmem((TILES, 128, 256), BF16),
            vmem((TILES, 128, 256), BF16),
            vmem((2, 128, 1024), BF16),
            vmem((2, 128, 1024), BF16),
            vmem((2 * TOK, 256), BF16),
            vmem((2, GRP, 64), F32),
            pltpu.SMEM((32,), F32),
            vmem((2, GRP, 64, 16), F32),
            vmem((2, GRP, 16, 64), F32),
            vmem((1, 256), F32),
            vmem((512, 16), BF16),
            vmem((512, 16), BF16),
            vmem((16, 4, 8, 128), F32),
            vmem((4, 8, 128), F32),
            vmem((TOK, 256), BF16),
            vmem((2, TOK, 256), BF16),
            vmem((TOK, 2048), BF16),
            dma((12,)),
            dma((6 * PER_ITEM,)),
            dma((6 * PER_ITEM,)),
            dma, dma, dma, dma,
            dma((16,)),
            dma((16,)),
            dma, dma,
            dma((16,)),
            dma((16,)),
            dma((8,)),
        ],
        compiler_params=pltpu.CompilerParams(
            collective_id=0, has_side_effects=True, vmem_limit_bytes=48 * 1024 * 1024
        ),
    )(hid, win, lamr, lami, lst, br, bi, cr, ci, skip.reshape(1, 512), lin, gate)


def solution(mesh):
    placed = (
        P("dp", "sp", None),
        P(("sp", "dp"), None),
        *(P(),) * 8,
        P(None, ("sp", "dp")),
        P(None, ("sp", "dp")),
    )
    return jax.shard_map(
        shards, mesh=mesh, in_specs=placed, out_specs=P("dp", "sp", None), check_vma=False
    )
```

time: 269 us -> 47.6 us (0.18)
  local copies, waits for them, and re-layouts: 127 us -> 4.29 us
  waiting for transfers between devices: 74.2 us -> 0 us
  Pallas kernels: 0 us -> 42.9 us
  other arithmetic: 19.4 us -> 0 us
  between operations: 13.5 us -> 0.16 us
  matrix products: 13.3 us -> 0 us
  blocking collectives: 9.92 us -> 0 us
  loops' own time: 5.28 us -> 0 us
  starting transfers between devices: 4.08 us -> 0 us
    slice x250 -> x0, local copies, waits for them, and re-layouts: 112 us -> none  [block_scan(): lax.associative_scan(combine, (are, aim, drive_re, drive_im), axis=0)]
    all_gather x1 -> x0, waiting for transfers between devices: 70.3 us -> none  [rows_first(): out = lax.all_gather(both, axis, axis=0, tiled=True)]
    pallas_call x0 -> x1, Pallas kernels: none -> 42.9 us  [shards(): pl.pallas_call(kernel, name='mixer', out_shape=jax.ShapeDtypeStruct((1, T...]
    dot_general x19 -> x0, matrix products: 13.3 us -> none  [the longest x1 3.24 us: shards(): linear = jnp.dot(mixer_out, whole_lin, preferred_element_type=jnp.float32)]
    all_to_all x1 -> x0, blocking collectives: 9.92 us -> none  [shards(): lax.all_to_all(mixer_local, 'sp', split_axis=0, concat_axis=1, tiled=True)]
    add x211 -> x0, other arithmetic: 8.74 us -> none  [the longest x120 3.4 us: block_scan(): lax.associative_scan(combine, (are, aim, drive_re, drive_im), axis=0)]
    another operation x1 -> x0, loops' own time: 5.28 us -> none  [run_blocks(): _, results = lax.scan(block_step, start, blocks)]
    concatenate x129 -> x0, other arithmetic: 5.18 us -> none  [the longest x128 3.75 us: block_scan(): lax.associative_scan(combine, (are, aim, drive_re, drive_im), axis=0)]
  transfers between devices with their start and end apart: 2 -> 0, of which waited for: 2 -> 0; matrix products, arithmetic and copies ran while one was open for 3% -> 0% of each run, Pallas kernels for 0% -> 0%
where the time goes in v1:
time: 47.6 us; the launch traced here: 47.3 us
  Pallas kernels  42.9 us (90%)
  local copies, waits for them, and re-layouts  4.29 us (9%)
    pallas_call x1, Pallas kernels, shards(): pl.pallas_call(kernel, name='mixer', out_shape=jax.ShapeDtypeStruct((1, T...  42.9 us
    unnamed x23, local copies, waits for them, and re-layouts  4.29 us

profile of v1, /device:TPU:1, one launch (start us, length us, event | category | flops | bytes accessed | tf_op | source)
XLA Modules:
  0.0 47.3 jit_solution(7186559257344061337)
XLA Ops:
  0.0 0.0 copy-start.8
  0.0 0.9 %copy.15.lin = bf16[512,16]{1,0:T(8,128)(2,1)S(1)} copy(bf16[512,16]{0,1:T(8,128)(2,1)} %param.22) | data formatting | bytes 32768 | tf_op args[10]
  0.9 0.8 %copy.16.gate = bf16[512,16]{1,0:T(8,128)(2,1)S(1)} copy(bf16[512,16]{0,1:T(8,128)(2,1)} %param.23) | data formatting | bytes 32768 | tf_op args[11]
  1.7 0.0 copy-done.8
  1.7 0.3 copy.13.br
  2.1 0.0 copy-start
  2.1 0.0 copy-start.1
  2.1 0.0 copy-start.2
  2.1 0.0 copy-start.3
  2.1 0.0 copy-start.4
  2.2 0.0 copy-start.5
  2.2 0.0 copy-start.6
  2.2 0.0 copy-start.7
  2.2 1.4 %copy.14.bi = f32[32,64,16]{2,1,0:T(8,128)S(1)} copy(f32[32,64,16]{1,2,0:T(8,128)} %param.18) | data formatting | bytes 262144 | tf_op args[6]
  3.6 0.0 copy-done
  3.6 0.0 copy-done.1
  3.6 0.0 copy-done.2
  3.6 0.0 copy-done.3
  3.6 0.0 copy-done.4
  3.6 0.0 copy-done.5
  3.6 0.0 copy-done.6
  3.6 0.0 copy-done.7
  3.6 42.9 %mixer.1 = bf16[1,128,2048]{2,1,0:T(8,128)(2,1)S(1)} custom-call(bf16[1,128,2048]{2,1,0:T(8,128)(2,1)S(1)} %copy-done, bf16[16,512]{1,0:T(8,128)(2,1)S(1)} %copy-done.3, f32[32,64]{1,0:T(8,128)S(1)} %copy-done.4, f32[32,64]{1,0:T(8,128)S(1)} %copy-done.5, f32[32]{0:T(128)S(1)} %copy-done.7, f32[32,64,16]{2,1,0:T(8,128)S(1)} %copy.13.br, ...), custom_call_target="tpu_custom_call" | custom-call | tf_op jit(solution)/shard_map/mixer/pallas_call | solution.py:381
  46.5 0.8 %copy.18 = bf16[1,128,2048]{2,1,0:T(8,128)(2,1)} copy(bf16[1,128,2048]{2,1,0:T(8,128)(2,1)S(1)} %mixer.1) | data formatting | bytes 1048576
Async XLA Ops:
  0.0 1.7 %copy-start.8 = (f32[32,64,16]{1,2,0:T(8,128)S(1)}, f32[32,64,16]{1,2,0:T(8,128)}, u32[]{:S(2)}) copy-start(f32[32,64,16]{1,2,0:T(8,128)} %param.17) | copy-start | bytes 393220
  2.1 1.5 %copy-start = (bf16[1,128,2048]{2,1,0:T(8,128)(2,1)S(1)}, bf16[1,128,2048]{2,1,0:T(8,128)(2,1)}, u32[]{:S(2)}) copy-start(bf16[1,128,2048]{2,1,0:T(8,128)(2,1)} %hid.1) | copy-start | bytes 1572868
  2.1 1.5 %copy-start.1 = (f32[32,16,64]{2,1,0:T(8,128)S(1)}, f32[32,16,64]{2,1,0:T(8,128)}, u32[]{:S(2)}) copy-start(f32[32,16,64]{2,1,0:T(8,128)} %cr.1) | copy-start | bytes 393220
  2.1 1.5 %copy-start.2 = (f32[32,16,64]{2,1,0:T(8,128)S(1)}, f32[32,16,64]{2,1,0:T(8,128)}, u32[]{:S(2)}) copy-start(f32[32,16,64]{2,1,0:T(8,128)} %ci.1) | copy-start | bytes 393220
  2.1 1.5 %copy-start.3 = (bf16[16,512]{1,0:T(8,128)(2,1)S(1)}, bf16[16,512]{1,0:T(8,128)(2,1)}, u32[]{:S(2)}) copy-start(bf16[16,512]{1,0:T(8,128)(2,1)} %win.1) | copy-start | bytes 49156
  2.1 1.5 %copy-start.4 = (f32[32,64]{1,0:T(8,128)S(1)}, f32[32,64]{1,0:T(8,128)}, u32[]{:S(2)}) copy-start(f32[32,64]{1,0:T(8,128)} %lamr.1) | copy-start | bytes 24580
  2.2 1.5 %copy-start.5 = (f32[32,64]{1,0:T(8,128)S(1)}, f32[32,64]{1,0:T(8,128)}, u32[]{:S(2)}) copy-start(f32[32,64]{1,0:T(8,128)} %lami.1) | copy-start | bytes 24580
  2.2 1.5 %copy-start.6 = (f32[512]{0:T(512)S(1)}, f32[512]{0:T(512)}, u32[]{:S(2)}) copy-start(f32[512]{0:T(512)} %param.21) | copy-start | bytes 6148
  2.2 1.5 %copy-start.7 = (f32[32]{0:T(128)S(1)}, f32[32]{0:T(128)}, u32[]{:S(2)}) copy-start(f32[32]{0:T(128)} %lst.1) | copy-start | bytes 388

commit v2 on v1

v2 whole, which is shorter than its diff:
```python
import functools

import jax
import jax.numpy as jnp
from jax import lax
from jax.experimental import pallas as pl
from jax.experimental.pallas import tpu as pltpu
from jax.sharding import PartitionSpec as P

MESH = pl.DeviceIdType.MESH
ANY = pl.ANY
HIGH = lax.Precision.HIGHEST
NT = (((1,), (1,)), ((), ()))
F32, BF16 = jnp.float32, jnp.bfloat16

TOK = 128
GRP = 16
TILES = 8
STR = 136
SEQ = 2 * TILES * STR

ITEMS = ((0, (1, 2, 0)), (256, (0, 2, 1)))
PER_ITEM = 12


def split(a):
    high = a.astype(BF16)
    return high, (a - high.astype(F32)).astype(BF16)


def kernel(
    hid, win, lamr, lami, lst, br, bi, cr, ci, skip, lin, gate, out,
    hbuf, wbuf, lbuf, gbuf, drive, bh, bl, ch, cl, ubuf,
    lamv, lstv, bv, cv, skv, wsend, fact, fbuf, fsend, msend, mbuf,
    loc, rs, rr, hs, hr, ws, wr, ls, lr, fs, fr, ms, mr, ds_, dr_,
):
    scopes = []

    def phase(name):
        if scopes:
            scopes.pop().__exit__(None, None, None)
        if name:
            scopes.append(jax.named_scope(name))
            scopes[-1].__enter__()

    phase("loads")
    sp, dp = lax.axis_index("sp"), lax.axis_index("dp")
    z, x, y, h = lax.div(sp, 4), lax.rem(sp, 4), lax.div(dp, 2), lax.rem(dp, 2)
    at = (z, x, y)
    other = 1 - h
    peer = (sp, y * 2 + other)

    def device(pos):
        return (pos[0] * 4 + pos[1], pos[2] * 2 + h)

    def moved(axis, by):
        pos = list(at)
        pos[axis] = lax.rem(at[axis] + by + 4, 4)
        return device(pos)

    def remote(src, dst, send, recv, to):
        return pltpu.make_async_remote_copy(
            src_ref=src, dst_ref=dst, send_sem=send, recv_sem=recv, device_id=to, device_id_type=MESH
        )

    half_rows = pl.ds(h * GRP, GRP)
    half_cols = pl.ds(pl.multiple_of(h * 256, 256), 256)
    other_cols = pl.ds(pl.multiple_of(other * 256, 256), 256)
    loads = [
        (win.at[:, half_cols], wbuf.at[z, x, y, h]),
        (win.at[:, other_cols], wsend),
        (lin, lbuf.at[z, x, y, h]),
        (gate, gbuf.at[z, x, y, h]),
        (hid.at[0], hbuf.at[h]),
        (lamr.at[half_rows], lamv.at[0]),
        (lami.at[half_rows], lamv.at[1]),
        (br.at[half_rows], bv.at[0]),
        (bi.at[half_rows], bv.at[1]),
        (cr.at[half_rows], cv.at[0]),
        (ci.at[half_rows], cv.at[1]),
        (skip.at[:, half_cols], skv),
        (lst, lstv),
    ]
    loads = [pltpu.make_async_copy(s, d, loc.at[k]) for k, (s, d) in enumerate(loads)]
    for c in loads:
        c.start()

    phase("barrier")
    def place(dz, dx, dy, core):
        return (
            lax.rem(z + dz, 4) * 4 + lax.rem(x + dx, 4),
            lax.rem(y + dy, 4) * 2 + core,
        )

    def in_plane(i, j, core):
        return place(h * i, other * i, j, core)

    senders = [place(0, i, j, 0) for i in range(4) for j in range(4)]
    senders += [place(i, 0, j, 1) for i in range(4) for j in range(4)]
    senders += [
        place(other * i + h * j, other * j + h * i, 0, h) for i in range(1, 4) for j in range(4)
    ]
    barrier = pltpu.get_barrier_semaphore()
    for to in senders:
        pl.semaphore_signal(barrier, inc=1, device_id=to, device_id_type=MESH)
    pl.semaphore_wait(barrier, len(senders))

    def slab(item, phase, i, cols=None):
        first, order = ITEMS[item]
        idx = [at[a] for a in range(3)]
        for a in order[: phase - 1]:
            idx[a] = slice(None)
        idx[order[phase - 1]] = i
        start, width = cols if cols is not None else (0, 256)
        return gbuf.at[idx[0], idx[1], idx[2], h, :, pl.ds(first + start, width)]

    def turn(axis, by):
        return lax.rem(at[axis] + by + 4, 4)

    def direct(item, phase):
        axis = ITEMS[item][1][phase - 1]
        copies = []
        for k in range(1, 4):
            sem = item * PER_ITEM + (phase - 1) * 3 + k - 1
            own = slab(item, phase, at[axis])
            copies.append(remote(own, own, rs.at[sem], rr.at[sem], moved(axis, k)))
        return copies

    H0, H1 = (0, 128), (128, 128)

    def last(item):
        axis = ITEMS[item][1][2]
        sem = item * PER_ITEM + 6
        plan = (
            (0, H0, 1), (0, H1, -1), (0, H1, 1), (0, H0, -1), (-1, H0, 1), (1, H1, -1),
        )
        copies = []
        for k, (which, cols, by) in enumerate(plan):
            piece = slab(item, 3, turn(axis, which), cols)
            copies.append(remote(piece, piece, rs.at[sem + k], rr.at[sem + k], moved(axis, by)))
        return copies

    first, second, third = {}, {}, {}
    for i in range(2):
        first[i], second[i], third[i] = direct(i, 1), direct(i, 2), last(i)

    passed = {}

    def pass_on(piece):
        sem = len(passed)
        passed[sem] = remote(piece, piece, ds_.at[sem], dr_.at[sem], peer)
        passed[sem].start()

    def pass_gate(item, which):
        pass_on(slab(item, 3, turn(ITEMS[item][1][2], which)))

    def pass_lin(which):
        pass_on(lbuf.at[:, :, turn(2, which), h])

    def start(copies):
        for c in copies:
            c.start()

    def arrived(copies):
        for c in copies:
            c.wait_recv()

    phase("first")
    loads[0].wait()
    loads[1].wait()
    own = wbuf.at[z, x, y, h]
    plane = []
    for j, i in sorted(((j, i) for j in range(4) for i in range(4)), key=lambda p: min(p[0], 1) + min(p[1], 1)):
        for core, src in ((h, own), (other, wsend)):
            if i + j > 0 or src is wsend:
                k = len(plane)
                slot = h * 16 + i * 4 + j
                plane.append(remote(src, own, ws.at[k], wr.at[slot], in_plane(i, j, core)))
                plane[-1].start()
    loads[2].wait()
    loads[3].wait()
    for i in range(2):
        start(first[i])
    lin_own = lbuf.at[z, x, y, h]
    lin_plane = [
        remote(lin_own, lin_own, ls.at[4 * i + j], lr.at[4 * i + j], place(i, j, 0, h))
        for i in range(4)
        for j in range(4)
        if i + j > 0
    ]
    start(lin_plane)
    loads[4].wait()
    h_pair = remote(hbuf.at[h], hbuf.at[h], hs, hr, peer)
    h_pair.start()

    def chunk(item, i, away):
        inner = lax.rem(at[1 - item] - i + 4, 4)
        final = lax.rem(at[item] + away + 4, 4)
        return wbuf.at[final, inner, :, item] if item == 0 else wbuf.at[inner, final, :, item]

    def to_neighbour(item, i, away, by, sem):
        piece = chunk(item, i, away)
        sem = item * PER_ITEM + sem
        return remote(piece, piece, rs.at[2 * PER_ITEM + sem], rr.at[2 * PER_ITEM + sem], moved(item, by))

    def lin_chunk(c, away, by, sem):
        piece = lbuf.at[:, :, turn(2, away), h, :, pl.ds(128 * c, 128)]
        return remote(piece, piece, ls.at[sem], lr.at[sem], moved(2, by))

    lin_up = [lin_chunk(c, 0, 1, 16 + c) for c in range(4)]
    lin_down = [lin_chunk(c, 0, -1, 20 + c) for c in range(4)]
    lin_far = [lin_chunk(c, -1, 1, 24 + c) for c in (0, 1)] + [lin_chunk(c, 1, -1, 24 + c) for c in (2, 3)]

    up = {(t, i): to_neighbour(t, i, 0, 1, i) for t in range(2) for i in range(4)}
    down = {(t, i): to_neighbour(t, i, 0, -1, 4 + i) for t in range(2) for i in range(4)}
    further = {(t, i): to_neighbour(t, i, -1, 1, 8 + i) for t in range(2) for i in (0, 1)}
    further.update({(t, i): to_neighbour(t, i, 1, -1, 8 + i) for t in range(2) for i in (3, 2)})

    def plane_arrived(item, i):
        for j in range(4):
            slot = item * 16 + i * 4 + j
            if i + j > 0:
                remote(own, own, ws.at[0], wr.at[slot], peer).wait_recv()

    phase("factors")
    for c in loads[5:]:
        c.wait()
    rows_g = lax.broadcasted_iota(jnp.int32, (GRP, 64), 0)
    log_step = jnp.zeros((GRP, 64), F32)
    for g in range(GRP):
        log_step = jnp.where(rows_g == g, lstv[h * GRP + g], log_step)
    lam_re, lam_im = lamv[0], lamv[1]
    step = jnp.exp(log_step)
    xpart = lam_re * step
    wpart = lam_im * step
    ex = jnp.exp(xpart)
    cosw, sinw, sinh_ = jnp.cos(wpart), jnp.sin(wpart), jnp.sin(0.5 * wpart)
    plain = ex == 1.0
    em1 = jnp.where(plain, xpart, (ex - 1.0) * xpart / jnp.log(jnp.where(plain, 2.0, ex)))
    num_re = em1 * cosw - 2.0 * sinh_ * sinh_
    num_im = ex * sinw
    size = lam_re * lam_re + lam_im * lam_im
    ratio_re = (num_re * lam_re + num_im * lam_im) / size
    ratio_im = (num_im * lam_re - num_re * lam_im) / size
    fact[0], fact[1] = ex * cosw, num_im

    def pairs(k):
        both = [fact[k, pl.ds(q, 8, stride=2), :] for q in range(2)]
        return jnp.concatenate(both, axis=1)

    a_re, a_im = pairs(0), pairs(1)
    p_re, p_im = a_re, a_im
    for _ in range(7):
        p_re, p_im = p_re * p_re - p_im * p_im, 2.0 * p_re * p_im

    phase("tables_b")
    rows_c = lax.broadcasted_iota(jnp.int32, (128, 128), 0)
    lanes_c = lax.broadcasted_iota(jnp.int32, (128, 128), 1)
    same = lax.rem(lax.div(rows_c, 16), 2) == lax.div(lanes_c, 64)
    pair_of = lax.div(rows_c, 32)

    def widened(part):
        part = part.reshape(128, 64)
        return jnp.where(same, jnp.concatenate([part, part], axis=1), 0.0)

    for a in range(2):
        groups = slice(8 * a, 8 * a + 8)
        r_re, r_im = ratio_re[groups].reshape(8, 1, 64), ratio_im[groups].reshape(8, 1, 64)
        b_re, b_im = bv[0, groups], bv[1, groups]
        for k, part in enumerate((r_re * b_re - r_im * b_im, r_re * b_im + r_im * b_re)):
            part = widened(part)
            for j in range(4):
                cols = slice(128 * k, 128 * k + 128)
                bh[4 * a + j, :, cols], bl[4 * a + j, :, cols] = split(jnp.where(pair_of == j, part, 0.0))

    phase("tables_c")
    for a in range(2):
        for k, sign in ((0, 1.0), (1, -1.0)):
            c = widened(cv[k, 8 * a : 8 * a + 8]) * sign
            for j in range(4):
                cols = slice(256 * j + 128 * k, 256 * j + 128 * k + 128)
                ch[a, :, cols], cl[a, :, cols] = split(jnp.where(pair_of == j, c, 0.0))

    phase("plane")
    remote(own, own, ws.at[0], wr.at[other * 16], peer).wait_recv()
    for i in (0, 1, 3, 2):
        for t in range(2):
            plane_arrived(t, i)
            up[t, i].start()
            down[t, i].start()
    phase("second")
    for i in range(2):
        arrived(first[i])
        start(second[i])
    phase("third_l")
    arrived(lin_plane)
    for c in range(4):
        lin_up[c].start()
        lin_down[(c + 2) % 4].start()
    pass_lin(0)
    phase("pass_w")
    for i in (0, 1, 3, 2):
        for t in range(2):
            (up if i in (0, 1) else down)[t, i].wait_recv()
            further[t, i].start()
    phase("third_g")
    for i in range(2):
        arrived(second[i])
        start(third[i][:2])
    for i in range(2):
        start(third[i][2:4])
        pass_gate(i, 0)
    phase("rest_w")
    for i in (0, 1, 3, 2):
        for t in range(2):
            (down if i in (0, 1) else up)[t, i].wait_recv()
    for i in (0, 1, 3, 2):
        for t in range(2):
            further[t, i].wait_recv()

    def forward_lin(c):
        (lin_up if c < 2 else lin_down)[c].wait_recv()
        lin_far[c].start()

    phase("inputs")
    h_pair.wait_recv()
    u = jnp.dot(
        hbuf[...].reshape(2 * TOK, 2048), wbuf[...].reshape(2048, 256), preferred_element_type=F32
    ).astype(BF16)
    ubuf[...] = u
    phase("drive")
    forward_lin(0)
    forward_lin(2)
    for j in range(TILES):
        cols = u[:, 128 * (j // 4) : 128 * (j // 4) + 128]
        d = jnp.dot(cols, bh[j], preferred_element_type=F32)
        d += jnp.dot(cols, bl[j], preferred_element_type=F32)
        for s in range(2):
            for k in range(2):
                rows = pl.ds(s * SEQ + (k * TILES + j) * STR, TOK)
                drive[rows, :] = d[TOK * s : TOK * s + TOK, 128 * k : 128 * k + 128]

    def scan(init, keep):
        def body(i, carry):
            carry = list(carry)
            for n in range(8):
                t = i * 8 + n
                for s in range(2):
                    at_re = pl.ds(s * SEQ + t, TILES, stride=STR)
                    at_im = pl.ds(s * SEQ + TILES * STR + t, TILES, stride=STR)
                    re, im = carry[2 * s], carry[2 * s + 1]
                    carry[2 * s] = a_re * re - a_im * im + drive[at_re, :]
                    carry[2 * s + 1] = a_re * im + a_im * re + drive[at_im, :]
                    if keep:
                        drive[at_re, :] = carry[2 * s]
                        drive[at_im, :] = carry[2 * s + 1]
            return tuple(carry)

        return lax.fori_loop(0, TOK // 8, body, init)

    phase("scan1")
    zero = jnp.zeros((8, 128), F32)
    ends = scan((zero,) * 4, False)
    for k in range(4):
        fsend[k] = ends[k]

    def to_later(k):
        return remote(fsend, fbuf.at[sp], fs.at[k], fr.at[sp], (lax.rem(sp + k, 16), dp))

    for k in range(1, 16):

        @pl.when(sp + k < 16)
        def _():
            to_later(k).start()

    phase("pass_l")
    forward_lin(1)
    forward_lin(3)
    for i in range(2):
        for k in (0, 1):
            third[i][k].wait_recv()
            third[i][4 + k].start()
    arrived(lin_up[2:])
    pass_lin(-1)
    arrived(lin_down[:2])
    pass_lin(1)
    for i in range(2):
        arrived(third[i][2:4])
        pass_gate(i, -1)
        pass_gate(i, 1)

    phase("fold")
    def fold(j, carry):
        remote(fsend, fbuf.at[j], fs.at[0], fr.at[j], peer).wait_recv()
        new = []
        for s in range(2):
            re, im = carry[2 * s], carry[2 * s + 1]
            new.append(p_re * re - p_im * im + fbuf[j, 2 * s])
            new.append(p_re * im + p_im * re + fbuf[j, 2 * s + 1])
        return tuple(new)

    begin = lax.fori_loop(0, sp, fold, (zero,) * 4)
    phase("scan2")
    scan(begin, True)
    phase("output")

    for a in range(2):
        tiles = []
        for j in range(4):
            for k in range(2):
                rows = [pl.ds(s * SEQ + (k * TILES + 4 * a + j) * STR, TOK) for s in range(2)]
                tiles.append(jnp.concatenate([drive[r, :] for r in rows], axis=0))
        s_high, s_low = split(jnp.concatenate(tiles, axis=1))
        summed = lax.dot_general(s_high, ch[a], NT, preferred_element_type=F32)
        summed += lax.dot_general(s_low, ch[a], NT, preferred_element_type=F32)
        summed += lax.dot_general(s_high, cl[a], NT, preferred_element_type=F32)
        cols = slice(128 * a, 128 * a + 128)
        mixer = jax.nn.gelu(summed + skv[:, cols] * ubuf[:, cols].astype(F32)).astype(BF16)
        mine = jnp.where(h == 0, mixer[:TOK].astype(F32), mixer[TOK:].astype(F32)).astype(BF16)
        theirs = jnp.where(h == 0, mixer[TOK:].astype(F32), mixer[:TOK].astype(F32)).astype(BF16)
        mbuf[h, :, cols] = mine
        msend[:, cols] = theirs
    m_pair = remote(msend, mbuf.at[h], ms, mr, peer)
    m_pair.start()

    phase("rest_l")
    arrived(lin_far)
    pass_lin(2)
    for i in range(2):
        arrived(third[i][4:])
        pass_gate(i, 2)
    phase("wait_m")
    m_pair.wait_recv()
    for sem in sorted(passed):
        passed[sem].wait_recv()

    m = jnp.concatenate([mbuf[0], mbuf[1]], axis=1)
    phase("project")
    for n in range(8):
        rows = (n // 2, slice(2 * (n % 2), 2 * (n % 2) + 2))
        linear = lax.dot_general(m, lbuf[rows].reshape(256, 512), NT, preferred_element_type=F32)
        gated = lax.dot_general(m, gbuf[rows].reshape(256, 512), NT, preferred_element_type=F32)
        out[0, :, 256 * n : 256 * n + 256] = (linear * jax.nn.sigmoid(gated)).astype(BF16)

    phase("sent")
    for i in range(2):
        for c in first[i] + second[i] + third[i]:
            c.wait_send()
    for c in lin_plane + lin_up + lin_down + lin_far:
        c.wait_send()
    for c in plane + list(up.values()) + list(down.values()) + list(further.values()):
        c.wait_send()
    for sem in sorted(passed):
        passed[sem].wait_send()
    for c in (h_pair, m_pair):
        c.wait_send()
    for k in range(1, 16):

        @pl.when(sp + k < 16)
        def _():
            to_later(k).wait_send()

    phase(None)


def shards(hid, win, lamr, lami, lst, br, bi, cr, ci, skip, lin, gate):
    br, bi = jnp.swapaxes(br, 1, 2), jnp.swapaxes(bi, 1, 2)
    operands = (hid, win, lamr, lami, lst, br, bi, cr, ci, skip.reshape(1, 512), lin.T, gate.T)
    operands = [pltpu.with_memory_space_constraint(a, pltpu.HBM) for a in operands]
    dma = pltpu.SemaphoreType.DMA
    vmem = pltpu.VMEM
    return pl.pallas_call(
        kernel,
        name="mixer",
        out_shape=vmem((1, TOK, 2048), BF16),
        in_specs=[pl.BlockSpec(memory_space=pltpu.HBM)] * 12,
        out_specs=pl.BlockSpec(memory_space=vmem),
        scratch_shapes=[
            vmem((2, TOK, 2048), BF16),
            vmem((4, 4, 4, 2, 16, 256), BF16),
            vmem((4, 4, 4, 2, 16, 512), BF16),
            vmem((4, 4, 4, 2, 16, 512), BF16),
            vmem((2 * SEQ, 128), F32),
            vmem((TILES, 128, 256), BF16),
            vmem((TILES, 128, 256), BF16),
            vmem((2, 128, 1024), BF16),
            vmem((2, 128, 1024), BF16),
            vmem((2 * TOK, 256), BF16),
            vmem((2, GRP, 64), F32),
            pltpu.SMEM((32,), F32),
            vmem((2, GRP, 16, 64), F32),
            vmem((2, GRP, 16, 64), F32),
            vmem((1, 256), F32),
            vmem((16, 256), BF16),
            vmem((2, GRP, 64), F32),
            vmem((16, 4, 8, 128), F32),
            vmem((4, 8, 128), F32),
            vmem((TOK, 256), BF16),
            vmem((2, TOK, 256), BF16),
            dma((13,)),
            dma((4 * PER_ITEM,)),
            dma((4 * PER_ITEM,)),
            dma, dma,
            dma((31,)),
            dma((32,)),
            dma((28,)),
            dma((28,)),
            dma((16,)),
            dma((16,)),
            dma, dma,
            dma((16,)),
            dma((16,)),
        ],
        compiler_params=pltpu.CompilerParams(
            collective_id=0, has_side_effects=True, vmem_limit_bytes=48 * 1024 * 1024
        ),
    )(*operands)


def solution(mesh):
    placed = (
        P("dp", "sp", None),
        P(("sp", "dp"), None),
        *(P(),) * 8,
        P(None, ("sp", "dp")),
        P(None, ("sp", "dp")),
    )
    return jax.shard_map(
        shards, mesh=mesh, in_specs=placed, out_specs=P("dp", "sp", None), check_vma=False
    )
```

time: 47.6 us -> 36.7 us (0.77)
  the two profiles are of different devices: /device:TPU:1 before, /device:TPU:33 now
where the time goes in v2:
time: 36.7 us; the launch traced here: 36.6 us
  Pallas kernels  35.8 us (98%)
  local copies, waits for them, and re-layouts  0.8 us (2%)
    pallas_call x1, Pallas kernels, shards(): pl.pallas_call(kernel, name='mixer', out_shape=vmem((1, TOK, 2048), BF16)...  35.8 us
    unnamed x1, local copies, waits for them, and re-layouts  0.8 us

profile of v2, /device:TPU:33, one launch (start us, length us, event | category | flops | bytes accessed | tf_op | source)
XLA Modules:
  0.0 36.6 jit_solution(6379820066706573500)
XLA Ops:
  0.0 35.8 %mixer.1 = bf16[1,128,2048]{2,1,0:T(8,128)(2,1)S(1)} custom-call(bf16[1,128,2048]{2,1,0:T(8,128)(2,1)} %hid.1, bf16[16,512]{1,0:T(8,128)(2,1)} %win.1, f32[32,64]{1,0:T(8,128)} %lamr.1, f32[32,64]{1,0:T(8,128)} %lami.1, f32[32]{0:T(128)} %lst.1, f32[32,16,64]{2,1,0:T(8,128)} %bitcast.5, f32[32,16,64]{2,1,0:T(8,128)} %bitcast.6, f32[32,16,64]{2,1,0:T(8,128)} %cr.1, ...), custom_call_target="tpu_custom_call" | custom-call | tf_op jit(solution)/shard_map/mixer/pallas_call | solution.py:472
  35.8 0.8 %copy.14 = bf16[1,128,2048]{2,1,0:T(8,128)(2,1)} copy(bf16[1,128,2048]{2,1,0:T(8,128)(2,1)S(1)} %mixer.1) | data formatting | bytes 1048576
